TPU v7x, 256 devices: a whole 4x4x8 slice. The times are simulated.
256 devices in a mesh: sp: 64 (over z, x, core), tp: 4 (over y).
Axes of the slice: x: 4, y: 4, z: 8, core: 2. Of those that a mesh axis runs over, the one named last changes fastest.
Arguments:
- residual: bfloat16 [16384, 2048], P('sp', 'tp'), may hold values from -8 to 8
- query_latent: bfloat16 [16384, 512], P('sp'), may hold values from -6 to 6
- shared_latent: bfloat16 [16384, 256], P('sp'), may hold values from -6 to 6
- rotary_key: bfloat16 [16384, 32], P('sp'), may hold values from -300 to 300
- query_gain: float32 [512], replicated, may hold values from 0.1 to 1.9
- latent_gain: float32 [256], replicated, may hold values from 0.1 to 1.9
- query_narrow: bfloat16 [512, 384], P(None, 'tp'), may hold values from -0.5 to 0.5
- key_narrow: bfloat16 [256, 256], P(None, 'tp'), may hold values from -0.375 to 0.375
- value_narrow: bfloat16 [256, 256], P(None, 'tp'), may hold values from -0.375 to 0.375
- query_wide: bfloat16 [512, 640], P(None, 'tp'), may hold values from -0.5 to 0.5
- key_wide: bfloat16 [256, 512], P(None, 'tp'), may hold values from -0.375 to 0.375
- value_wide: bfloat16 [256, 512], P(None, 'tp'), may hold values from -0.375 to 0.375
- output_narrow: bfloat16 [256, 2048], P('tp'), may hold values from -1.75 to 1.75
- output_wide: bfloat16 [512, 2048], P('tp'), may hold values from -1.75 to 1.75
- first_gain: float32 [2048], P('tp'), may hold values from 0.1 to 1.9
- first_bias: float32 [2048], P('tp'), may hold values from -1.5 to 1.5
- gate_weight: bfloat16 [2048, 5632], P('sp', 'tp'), may hold values from -0.125 to 0.125
- up_weight: bfloat16 [2048, 5632], P('sp', 'tp'), may hold values from -0.125 to 0.125
- down_weight: bfloat16 [5632, 2048], P('tp', 'sp'), may hold values from -0.078125 to 0.078125
- second_gain: float32 [2048], P('tp'), may hold values from 0.1 to 1.9
- second_bias: float32 [2048], P('tp'), may hold values from -1.5 to 1.5
Outputs:
- layer_out: bfloat16 [16384, 2048], P('sp', 'tp')
All inputs are finite; a program needn't handle non-finite values.
Results may differ from a plain program's by a relative error of at most 0.017.
The roundings to bfloat16 on the way count: a program that leaves them out, or rounds other values in their place, can miss the bound.
Values may be sent and summed in bfloat16 or wider, within the bound.
A program may use at most 192 MiB of HBM per device.

v0:
```python
import jax
import jax.numpy as jnp
from jax import lax
from jax.sharding import PartitionSpec as P

ROPE = 32
NOPE_A = 64
V_A = 64
NOPE_B = 128
V_B = 128
GRID_W = 64
EPS_ROOT = 1e-06
EPS_LAYER = 1e-05
THETA = 10000.0
DEEP_ALPHA = 2.0**0.25


def in_one_piece(arrays, axis, dim, along):
    ends, at = ([], 0)
    for a in arrays[:-1]:
        at += a.shape[along]
        ends.append(at)
    both = jnp.concatenate(arrays, axis=along)
    return tuple(jnp.split(lax.all_gather(both, axis, axis=dim, tiled=True), ends, axis=along))


def split_up(x, dim, size):
    before, after = (x.shape[:dim], x.shape[dim + 1 :])
    return jnp.moveaxis(x.reshape(*before, size, -1, *after), dim, 0)


def sum_at_owner(x, axis, dim):
    size = lax.axis_size(axis)
    pieces = lax.all_to_all(split_up(x, dim, size), axis, 0, 0, tiled=True)
    return jnp.sum(pieces.astype(jnp.float32), axis=0)


def sent_to_all(x, axis):
    copies = jnp.broadcast_to(x, (lax.axis_size(axis), *x.shape))
    return lax.all_to_all(copies, axis, split_axis=0, concat_axis=0, tiled=True)


def of_everyone(x, axis):
    return sent_to_all(x, axis).sum(axis=0)


def in_one(arrays, axis):
    ends = [0]
    for a in arrays:
        ends.append(ends[-1] + a.size)
    so_far = of_everyone(jnp.concatenate([a.ravel() for a in arrays]), axis)
    return tuple((so_far[b:e].reshape(a.shape) for a, b, e in zip(arrays, ends, ends[1:])))


def in_order(pieces, dim):
    shape = list(pieces.shape[1:])
    shape[dim] *= pieces.shape[0]
    return jnp.moveaxis(pieces, 0, dim).reshape(shape)


def collect(x, axis, dim):
    return in_order(sent_to_all(x, axis), dim)


def rotate(half_part, angle):
    lower, upper = jnp.split(half_part, 2, axis=-1)
    cosine = jnp.cos(angle)
    sine = jnp.sin(angle)
    return jnp.concatenate([lower * cosine - upper * sine, upper * cosine + lower * sine], axis=-1)


def turn_axial(values_in, positions):
    quarter = values_in.shape[-1] // 4
    freqs = THETA ** (-(2.0 * jnp.arange(quarter, dtype=jnp.float32)) / (2 * quarter))
    row_angle = (positions // GRID_W).astype(jnp.float32)[:, None, None] * freqs
    col_angle = (positions % GRID_W).astype(jnp.float32)[:, None, None] * freqs
    first_half, second_half = jnp.split(values_in, 2, axis=-1)
    return jnp.concatenate([rotate(first_half, row_angle), rotate(second_half, col_angle)], axis=-1)


def root_scale(latent, gain):
    floated = latent.astype(jnp.float32)
    return (
        floated * lax.rsqrt(jnp.mean(floated * floated, axis=-1, keepdims=True) + EPS_ROOT) * gain
    )


def make_query(normed, weight, plain_dim, positions):
    product = jnp.dot(normed, weight, preferred_element_type=jnp.float32)
    head_count = weight.shape[1] // (plain_dim + ROPE)
    product = product.reshape(product.shape[0], head_count, plain_dim + ROPE)
    turned = turn_axial(product[:, :, plain_dim:], positions)
    return jnp.concatenate([product[:, :, :plain_dim], turned], axis=-1).astype(jnp.bfloat16)


def fresh_state(row_count, head_count, value_dim):
    largest = jnp.full((head_count, row_count), -jnp.inf, jnp.float32)
    totals = jnp.zeros((head_count, row_count), jnp.float32)
    weighted = jnp.zeros((row_count, head_count, value_dim), jnp.float32)
    return (largest, totals, weighted)


def update(state_now, queries, key_rows, value_rows, rotary_rows, plain_dim):
    largest, totals, weighted = state_now
    score_scale = queries.shape[2] ** (-0.5)
    scores = jnp.einsum(
        "qhd,khd->hqk", queries[:, :, :plain_dim], key_rows, preferred_element_type=jnp.float32
    )
    scores = scores + jnp.einsum(
        "qhd,kd->hqk", queries[:, :, plain_dim:], rotary_rows, preferred_element_type=jnp.float32
    )
    scores = scores * score_scale
    new_largest = jnp.max(scores, axis=-1)
    factor = jnp.exp(largest - new_largest)
    raised = jnp.exp(scores - new_largest[:, :, None])
    totals = totals * factor + jnp.sum(raised, axis=-1)
    added = jnp.einsum(
        "hqk,khd->qhd", raised.astype(jnp.bfloat16), value_rows, preferred_element_type=jnp.float32
    )
    weighted = weighted * factor.T[:, :, None] + added
    return (new_largest, totals, weighted)


def finish(state_now):
    largest, totals, weighted = state_now
    output = (weighted / totals.T[:, :, None]).astype(jnp.bfloat16)
    return output.reshape(output.shape[0], output.shape[1] * output.shape[2])


def finish_norm(summed, sums, squares, gain, bias, width_total):
    center = sums / width_total
    spread = squares / width_total - center * center
    normed = (summed - center[:, None]) * lax.rsqrt(spread + EPS_LAYER)[:, None]
    return (normed * gain + bias).astype(jnp.bfloat16)


def body(
    residual,
    query_latent,
    shared_latent,
    rotary_key,
    query_gain,
    latent_gain,
    query_narrow,
    key_narrow,
    value_narrow,
    query_wide,
    key_wide,
    value_wide,
    output_narrow,
    output_wide,
    first_gain,
    first_bias,
    gate_weight,
    up_weight,
    down_weight,
    second_gain,
    second_bias,
):
    row_count = residual.shape[0]
    offset = lax.axis_index("sp") * row_count
    positions = offset + jnp.arange(row_count, dtype=jnp.int32)
    query_normed = root_scale(query_latent, query_gain).astype(jnp.bfloat16)
    narrow_queries = make_query(query_normed, query_narrow, NOPE_A, positions)
    wide_queries = make_query(query_normed, query_wide, NOPE_B, positions)
    narrow_heads = narrow_queries.shape[1]
    wide_heads = wide_queries.shape[1]
    start_state = (
        fresh_state(row_count, narrow_heads, V_A),
        fresh_state(row_count, wide_heads, V_B),
    )
    shard_rows = in_one_piece((shared_latent, rotary_key), "sp", 0, 1)
    latent_rows = shard_rows[0]
    normed = root_scale(latent_rows, latent_gain).astype(jnp.bfloat16)
    count = latent_rows.shape[0]
    narrow_keys = jnp.dot(normed, key_narrow, preferred_element_type=jnp.float32).astype(
        jnp.bfloat16
    )
    narrow_vals = jnp.dot(normed, value_narrow, preferred_element_type=jnp.float32).astype(
        jnp.bfloat16
    )
    wide_keys = jnp.dot(normed, key_wide, preferred_element_type=jnp.float32).astype(jnp.bfloat16)
    wide_vals = jnp.dot(normed, value_wide, preferred_element_type=jnp.float32).astype(jnp.bfloat16)
    key_positions = jnp.arange(count, dtype=jnp.int32)
    rotated = turn_axial(shard_rows[1].astype(jnp.float32)[:, None, :], key_positions)[
        :, 0, :
    ].astype(jnp.bfloat16)
    count = rotated.shape[0]
    narrow_state = update(
        start_state[0],
        narrow_queries,
        narrow_keys.reshape(count, narrow_heads, NOPE_A),
        narrow_vals.reshape(count, narrow_heads, V_A),
        rotated,
        NOPE_A,
    )
    wide_state = update(
        start_state[1],
        wide_queries,
        wide_keys.reshape(count, wide_heads, NOPE_B),
        wide_vals.reshape(count, wide_heads, V_B),
        rotated,
        NOPE_B,
    )
    narrow_out = finish(narrow_state)
    wide_out = finish(wide_state)
    terms = jnp.dot(narrow_out, output_narrow, preferred_element_type=jnp.float32)
    terms = terms + jnp.dot(wide_out, output_wide, preferred_element_type=jnp.float32)
    mixed = sum_at_owner(terms.astype(jnp.bfloat16), "tp", 1)
    width_total = mixed.shape[1] * lax.axis_size("tp")
    summed = DEEP_ALPHA * residual.astype(jnp.float32) + mixed
    sums, squares = in_one((jnp.sum(summed, axis=1), jnp.sum(summed * summed, axis=1)), "tp")
    normed_first = finish_norm(summed, sums, squares, first_gain, first_bias, width_total)
    full_rows = collect(normed_first, "tp", 1)
    shard_rows = in_one_piece((gate_weight, up_weight), "sp", 0, 1)
    gate_part = jnp.dot(full_rows, shard_rows[0], preferred_element_type=jnp.float32)
    lifted_part = jnp.dot(full_rows, shard_rows[1], preferred_element_type=jnp.float32)
    hidden = (jax.nn.silu(gate_part) * lifted_part).astype(jnp.bfloat16)
    feed_terms = jnp.dot(
        hidden,
        lax.all_gather(down_weight, "sp", axis=1, tiled=True),
        preferred_element_type=jnp.float32,
    )
    feed = sum_at_owner(feed_terms.astype(jnp.bfloat16), "tp", 1)
    summed_two = DEEP_ALPHA * normed_first.astype(jnp.float32) + feed
    sums_two, squares_two = in_one(
        (jnp.sum(summed_two, axis=1), jnp.sum(summed_two * summed_two, axis=1)), "tp"
    )
    return finish_norm(summed_two, sums_two, squares_two, second_gain, second_bias, width_total)


def solution(mesh):
    return jax.shard_map(
        body,
        mesh=mesh,
        in_specs=(
            P("sp", "tp"),
            P("sp", None),
            P("sp", None),
            P("sp", None),
            P(),
            P(),
            P(None, "tp"),
            P(None, "tp"),
            P(None, "tp"),
            P(None, "tp"),
            P(None, "tp"),
            P(None, "tp"),
            P("tp", None),
            P("tp", None),
            P("tp"),
            P("tp"),
            P("sp", "tp"),
            P("sp", "tp"),
            P("tp", "sp"),
            P("tp"),
            P("tp"),
        ),
        out_specs=P("sp", "tp"),
        check_vma=False,
    )
```

profile of v0, /device:TPU:8, one launch (start us, length us, event | category | flops | bytes accessed | tf_op | source)
XLA Modules:
  0.0 313.4 jit_solution(8049191181758371652)
XLA Ops:
  6.5 1.1 copy.41
  7.6 1.4 pad_maximum_fusion.4
  9.1 1.6 pad_maximum_fusion.1
  10.8 0.7 all-gather.8.cloned.1.call-update
  11.5 1.1 fusion.72
  12.6 1.3 convolution_bitcast_fusion.4
  13.9 1.3 convolution_bitcast_fusion.5
  15.4 84.6 %all-gather.4.cloned.1.call-done = bf16[16384,288]{0,1:T(8,128)(2,1)} async-done(((bf16[256,288]{0,1:T(8,128)(2,1)}), bf16[16384,288]{0,1:T(8,128)(2,1)}) %all-gather.4.cloned.1.call-update) | async-done | bytes 9437200 | tf_op jit(solution)/shard_map/all_gather | solution.py:24
  99.9 5.1 %fusion.4 = f32[16384]{0:T(1024)S(1)} fusion(bf16[16384,288]{0,1:T(8,128)(2,1)} %all-gather.4.cloned.1.call-done), kind=kLoop, calls=%fused_computation.14 | loop fusion | flops 12566528 | bytes 8454144 | tf_op jit(solution)/shard_map/reduce_sum | solution.py:84
  105.1 1.4 fusion.62
  106.5 4.4 %fusion.84 = (bf16[16384,8]{0,1:T(8,128)(2,1)S(1)}, bf16[16384,8]{0,1:T(8,128)(2,1)S(1)}, bf16[16384,8]{0,1:T(8,128)(2,1)S(1)}, bf16[16384,8]{0,1:T(8,128)(2,1)S(1)}) fusion(f32[16384,1,32]{0,2,1:T(8,128)S(1)} %fusion.62, f32[8]{0:T(128)S(1)} %multiply_power_fusion, f32[16384]{0:T(1024)S(1)} %get-tuple-element.43, f32[16384]{0:T(1024)S(1)} %get-tuple-element.44), kind=kLoop, calls=%fused_computation.90 | loop fusion | flops 2359296 | bytes 3276832 | tf_op jit(solution)/shard_map/concatenate | solution.py:78
  110.9 8.1 %convolution_bitcast_fusion.2 = f32[1,256,16384]{2,1,0:T(8,128)} fusion(bf16[16384,8]{0,1:T(8,128)(2,1)S(1)} %get-tuple-element.13, bf16[16384,8]{0,1:T(8,128)(2,1)S(1)} %get-tuple-element.14, bf16[16384,8]{0,1:T(8,128)(2,1)S(1)} %get-tuple-element.10, bf16[16384,8]{0,1:T(8,128)(2,1)S(1)} %get-tuple-element.9, bf16[256,1,8]{0,2,1:T(8,128)(2,1)S(1)} %get-tuple-element.25, ...), kind=kOutput, calls=%fused_computation.2 | convolution fusion | flops 272695296 | bytes 17842176 | tf_op jit(solution)/shard_map/qhd,kd->hqk/dot_general | solution.py:109
  119.0 14.3 %fusion.167 = (f32[256]{0:T(256)S(1)}, f32[1,256,16384]{2,1,0:T(8,128)}) fusion(f32[1,256,16384]{2,1,0:T(8,128)} %convolution_bitcast_fusion.2, bf16[256,64]{0,1:T(8,128)(2,1)S(1)} %copy-done.4, f32[256]{0:T(256)S(1)} %copy-done.5, f32[16384]{0:T(1024)S(1)} %add_rsqrt_fusion, bf16[16384,288]{0,1:T(8,128)(2,1)} %all-gather.4.cloned.1.call-done, ...), kind=kOutput, calls=%fused_computation.191 | convolution fusion | flops 1104150272 | bytes 42076160 | tf_op jit(solution)/shard_map/qhd,khd->hqk/dot_general | solution.py:106
  133.3 8.1 %convolution_bitcast_fusion = f32[1,256,16384]{2,1,0:T(8,128)} fusion(bf16[16384,8]{0,1:T(8,128)(2,1)S(1)} %get-tuple-element.13, bf16[16384,8]{0,1:T(8,128)(2,1)S(1)} %get-tuple-element.14, bf16[16384,8]{0,1:T(8,128)(2,1)S(1)} %get-tuple-element.10, bf16[16384,8]{0,1:T(8,128)(2,1)S(1)} %get-tuple-element.9, bf16[256,1,8]{0,2,1:T(8,128)(2,1)S(1)} %get-tuple-element.28, ...), kind=kOutput, calls=%fused_computation | convolution fusion | flops 272695296 | bytes 17842176 | tf_op jit(solution)/shard_map/qhd,kd->hqk/dot_general | solution.py:109
  141.4 8.2 %fusion.7 = f32[256]{0:T(256)S(1)} fusion(f32[1,256,16384]{2,1,0:T(8,128)} %get-tuple-element.42, f32[256]{0:T(256)S(1)} %get-tuple-element.41), kind=kLoop, calls=%fused_computation.19 | loop fusion | flops 8388352 | bytes 16779264 | tf_op jit(solution)/shard_map/reduce_sum | solution.py:116
  149.6 15.2 %fusion.164 = (f32[256]{0:T(256)S(1)}, f32[1,256,16384]{2,1,0:T(8,128)}) fusion(f32[1,256,16384]{2,1,0:T(8,128)} %convolution_bitcast_fusion, bf16[256,128]{1,0:T(8,128)(2,1)S(1)} %copy-done.3, f32[256]{0:T(256)S(1)} %copy-done.5, f32[16384]{0:T(1024)S(1)} %add_rsqrt_fusion, bf16[16384,288]{0,1:T(8,128)(2,1)} %all-gather.4.cloned.1.call-done, ...), kind=kOutput, calls=%fused_computation.190 | convolution fusion | flops 2178940672 | bytes 42141696 | tf_op jit(solution)/shard_map/qhd,khd->hqk/dot_general | solution.py:106
  164.8 8.5 %fusion.9 = f32[256]{0:T(256)S(1)} fusion(f32[1,256,16384]{2,1,0:T(8,128)} %get-tuple-element.40, f32[256]{0:T(256)S(1)} %get-tuple-element.39), kind=kLoop, calls=%fused_computation.21 | loop fusion | flops 8388352 | bytes 16779264 | tf_op jit(solution)/shard_map/reduce_sum | solution.py:116
  173.4 12.0 %fusion.44 = bf16[256,128]{0,1:T(8,128)(2,1)S(1)} fusion(f32[1,256,16384]{2,1,0:T(8,128)} %get-tuple-element.40, f32[256]{0:T(256)S(1)} %get-tuple-element.39, bf16[256,128]{1,0:T(8,128)(2,1)S(1)} %copy-done.10, f32[256]{0:T(256)S(1)} %get-tuple-element.38, f32[256]{0:T(256)S(1)} %get-tuple-element.37, f32[256]{0:T(256)S(1)} %copy-done.5, ...), kind=kOutput, calls=%fused_computation.46 | convolution fusion | flops 2174844928 | bytes 25366528 | tf_op jit(solution)/shard_map/hqk,khd->qhd/dot_general | solution.py:117
  185.4 0.5 fusion.170
  185.8 11.3 %fusion.59 = bf16[256,64]{0,1:T(8,128)(2,1)S(1)} fusion(f32[1,256,16384]{2,1,0:T(8,128)} %get-tuple-element.42, f32[256]{0:T(256)S(1)} %get-tuple-element.41, bf16[256,64]{0,1:T(8,128)(2,1)S(1)} %copy-done.11, f32[256]{0:T(256)S(1)} %get-tuple-element.36, f32[256]{0:T(256)S(1)} %get-tuple-element.35, f32[256]{0:T(256)S(1)} %copy-done.5, ...), kind=kOutput, calls=%fused_computation.51 | convolution fusion | flops 1100005376 | bytes 25300992 | tf_op jit(solution)/shard_map/hqk,khd->qhd/dot_general | solution.py:117
  197.2 0.5 fusion.26
  197.7 18.6 %all_to_all.27 = bf16[4,256,512]{2,1,0:T(8,128)(2,1)S(1)} all-to-all(bf16[4,256,512]{2,1,0:T(8,128)(2,1)S(1)} %bitcast.138), channel_id=1, replica_groups=mesh['sp'=64,'tp'=4] {'tp'}, dimensions={0} | all-to-all | bytes 2097152 | tf_op jit(solution)/shard_map/all_to_all | solution.py:34
  216.5 0.2 fusion.87
  216.8 7.7 %all_to_all.28 = f32[4,1,512]{2,1,0:T(1,128)S(1)} all-to-all(f32[4,1,512]{2,1,0:T(1,128)S(1)} %broadcast_in_dim.16), channel_id=1, replica_groups=mesh['sp'=64,'tp'=4] {'tp'}, dimensions={0} | all-to-all | bytes 16384 | tf_op jit(solution)/shard_map/all_to_all | solution.py:40
  224.9 15.6 %all_to_all.29 = bf16[4,256,512]{1,2,0:T(8,128)(2,1)S(1)} all-to-all(bf16[4,256,512]{1,2,0:T(8,128)(2,1)S(1)} %broadcast_in_dim.17), channel_id=1, replica_groups=mesh['sp'=64,'tp'=4] {'tp'}, dimensions={0} | all-to-all | bytes 2097152 | tf_op jit(solution)/shard_map/all_to_all | solution.py:40
  240.5 5.6 %fusion.21 = f32[256,1408]{1,0:T(8,128)} fusion(bf16[256,2048]{0,1:T(8,128)(2,1)S(1)} %bitcast.140, bf16[2048,2816]{1,0:T(8,128)(2,1)} %all-gather.6.cloned.1.call-done), kind=kOutput, calls=%fused_computation.31 | convolution fusion | flops 1476395008 | bytes 8257536 | tf_op jit(solution)/shard_map/dot_general | solution.py:216
  246.1 24.8 %all-gather.8.cloned.1.call-done = bf16[1408,2048]{0,1:T(8,128)(2,1)} async-done(((bf16[1408,32]{0,1:T(8,128)(2,1)}), bf16[1408,2048]{0,1:T(8,128)(2,1)}) %all-gather.8.cloned.1.call-update) | async-done | bytes 5767184 | tf_op jit(solution)/shard_map/all_gather | solution.py:221
  270.9 8.3 %convolution_convert_fusion.4 = bf16[256,2048]{1,0:T(8,128)(2,1)S(1)} fusion(bf16[1408,2048]{0,1:T(8,128)(2,1)} %all-gather.8.cloned.1.call-done, bf16[256,2048]{0,1:T(8,128)(2,1)S(1)} %bitcast.141, bf16[2048,2816]{1,0:T(8,128)(2,1)} %all-gather.6.cloned.1.call-done, f32[256,1408]{1,0:T(8,128)} %fusion.21), kind=kOutput, calls=%fused_computation.37 | convolution fusion | flops 2955476992 | bytes 15073280 | tf_op jit(solution)/shard_map/dot_general | solution.py:219
  279.3 18.7 %all_to_all.30 = bf16[4,256,512]{2,1,0:T(8,128)(2,1)S(1)} all-to-all(bf16[4,256,512]{2,1,0:T(8,128)(2,1)S(1)} %bitcast.139), channel_id=1, replica_groups=mesh['sp'=64,'tp'=4] {'tp'}, dimensions={0} | all-to-all | bytes 2097152 | tf_op jit(solution)/shard_map/all_to_all | solution.py:34
  298.1 0.2 fusion.88
  298.3 7.7 %all_to_all.31 = f32[4,1,512]{2,1,0:T(1,128)S(1)} all-to-all(f32[4,1,512]{2,1,0:T(1,128)S(1)} %broadcast_in_dim.18), channel_id=1, replica_groups=mesh['sp'=64,'tp'=4] {'tp'}, dimensions={0} | all-to-all | bytes 16384 | tf_op jit(solution)/shard_map/all_to_all | solution.py:40
  306.0 0.9 add_convert_fusion
  (53 shorter events, 1.4 us)
Async XLA Ops:
  6.5 178.8 %copy-start = (bf16[128,2048]{1,0:T(8,128)(2,1)S(1)}, bf16[128,2048]{1,0:T(8,128)(2,1)}, u32[]{:S(2)}) copy-start(bf16[128,2048]{1,0:T(8,128)(2,1)} %param.34) | copy-start | bytes 1572868
  6.5 93.4 %all-gather.4.cloned.1.call-start = ((), (), s32[]{:S(2)}) async-start(), calls=%async_computation.5 | async-start | bytes 9584640 | tf_op jit(solution)/shard_map/all_gather | solution.py:24
  9.0 231.5 %all-gather.6.cloned.1.call-start = ((), (), s32[]{:S(2)}) async-start(), calls=%async_computation.6 | async-start | bytes 11714560 | tf_op jit(solution)/shard_map/all_gather | solution.py:24
  10.7 260.2 %all-gather.8.cloned.1.call-start = ((), (), s32[]{:S(2)}) async-start(), calls=%async_computation.7 | async-start | bytes 5857280 | tf_op jit(solution)/shard_map/all_gather | solution.py:221
  110.8 8.1 %copy-start.4 = (bf16[256,64]{0,1:T(8,128)(2,1)S(1)}, bf16[256,64]{0,1:T(8,128)(2,1)}, u32[]{:S(2)}) copy-start(bf16[256,64]{0,1:T(8,128)(2,1)} %param.28) | copy-start | bytes 98308
  110.8 8.1 %copy-start.5 = (f32[256]{0:T(256)S(1)}, f32[256]{0:T(256)}, u32[]{:S(2)}) copy-start(f32[256]{0:T(256)} %param.26) | copy-start | bytes 3076
  141.4 8.2 %copy-start.3 = (bf16[256,128]{1,0:T(8,128)(2,1)S(1)}, bf16[256,128]{1,0:T(8,128)(2,1)}, u32[]{:S(2)}) copy-start(bf16[256,128]{1,0:T(8,128)(2,1)} %param.31) | copy-start | bytes 196612
  164.8 8.5 %copy-start.10 = (bf16[256,128]{1,0:T(8,128)(2,1)S(1)}, bf16[256,128]{1,0:T(8,128)(2,1)}, u32[]{:S(2)}) copy-start(bf16[256,128]{1,0:T(8,128)(2,1)} %param.32) | copy-start | bytes 196612
  173.4 12.5 %copy-start.11 = (bf16[256,64]{0,1:T(8,128)(2,1)S(1)}, bf16[256,64]{0,1:T(8,128)(2,1)}, u32[]{:S(2)}) copy-start(bf16[256,64]{0,1:T(8,128)(2,1)} %param.29) | copy-start | bytes 98308
  185.8 11.3 %copy-start.2 = (bf16[64,2048]{1,0:T(8,128)(2,1)S(1)}, bf16[64,2048]{1,0:T(8,128)(2,1)}, u32[]{:S(2)}) copy-start(bf16[64,2048]{1,0:T(8,128)(2,1)} %param.33) | copy-start | bytes 786436
  185.8 30.7 %copy-start.1 = (bf16[256,512]{1,0:T(8,128)(2,1)S(1)}, bf16[256,512]{1,0:T(8,128)(2,1)}, u32[]{:S(2)}) copy-start(bf16[256,512]{1,0:T(8,128)(2,1)} %param.21) | copy-start | bytes 786436
  197.2 27.3 %copy-start.6 = (f32[512]{0:T(512)S(1)}, f32[512]{0:T(512)}, u32[]{:S(2)}) copy-start(f32[512]{0:T(512)} %param.36) | copy-start | bytes 6148
  197.2 27.3 %copy-start.7 = (f32[512]{0:T(512)S(1)}, f32[512]{0:T(512)}, u32[]{:S(2)}) copy-start(f32[512]{0:T(512)} %param.35) | copy-start | bytes 6148
  246.1 59.9 %copy-start.8 = (f32[512]{0:T(512)S(1)}, f32[512]{0:T(512)}, u32[]{:S(2)}) copy-start(f32[512]{0:T(512)} %param.41) | copy-start | bytes 6148
  246.1 59.9 %copy-start.9 = (f32[512]{0:T(512)S(1)}, f32[512]{0:T(512)}, u32[]{:S(2)}) copy-start(f32[512]{0:T(512)} %param.40) | copy-start | bytes 6148
Sparse Core Ops, SparseCore 0:
  10.0 89.9 all-gather.3
  102.7 88.5 all-gather.5
  194.0 76.8 all-gather.7
where the time goes:
time: 314 us; the launch traced here: 313 us
  waiting for transfers between devices  110 us (35%)
  matrix products  86.3 us (27%)
  blocking collectives  68.2 us (22%)
  other arithmetic  33.7 us (11%)
  between operations  13.4 us (4%)
    all_gather x2, waiting for transfers between devices, in_one_piece(): lax.all_gather(both, axis, axis=dim, tiled=True)  84.6 us
    all_to_all x2, blocking collectives, sum_at_owner(): pieces = lax.all_to_all(split_up(x, dim, size), axis, 0, 0, tiled=True)  37.3 us
    all_to_all x3, blocking collectives, sent_to_all(): return lax.all_to_all(copies, axis, split_axis=0, concat_axis=0, tiled=True)  31 us
    dot_general x2, matrix products, update(): jnp.einsum('qhd,khd->hqk', queries[:, :, :plain_dim], key_rows, preferred...  29.5 us
    all_gather x1, waiting for transfers between devices, body(): lax.all_gather(down_weight, 'sp', axis=1, tiled=True)  24.8 us
    dot_general x2, matrix products, update(): jnp.einsum('hqk,khd->qhd', raised.astype(jnp.bfloat16), value_rows, prefe...  23.3 us
    reduce_sum x2, other arithmetic, update(): totals = totals * factor + jnp.sum(raised, axis=-1)  16.7 us
    dot_general x2, matrix products, update(): jnp.einsum('qhd,kd->hqk', queries[:, :, plain_dim:], rotary_rows, preferr...  16.2 us
  transfers between devices with their start and end apart: 3, of which 2 were waited for; matrix products, arithmetic and copies ran while one was open for 35% of the time, Pallas kernels for 0%

commit v1 on v0

--- a/solution.py
+++ b/solution.py
@@ -218,7 +218,9 @@
     hidden = (jax.nn.silu(gate_part) * lifted_part).astype(jnp.bfloat16)
     feed_terms = jnp.dot(
         hidden,
-        lax.all_gather(down_weight, "sp", axis=1, tiled=True),
+        jnp.concatenate(
+            lax.all_to_all(jnp.stack([down_weight] * lax.axis_size("sp")), "sp", 0, 0), axis=1
+        ),
         preferred_element_type=jnp.float32,
     )
     feed = sum_at_owner(feed_terms.astype(jnp.bfloat16), "tp", 1)

time: 314 us -> 427 us (1.36)
  waiting for transfers between devices: 110 us -> 210 us
  starting transfers between devices: 0.09 us -> 10.9 us
    all_to_all x0 -> x1, waiting for transfers between devices: none -> 124 us  [body(): lax.all_to_all(jnp.stack([down_weight] * lax.axis_size('sp')), 'sp', 0, 0)]
    all_gather x1 -> x0, waiting for transfers between devices: 24.8 us -> none  [body(): lax.all_gather(down_weight, 'sp', axis=1, tiled=True)]
    all_to_all x0 -> x1, starting transfers between devices: none -> 10.9 us  [body(): lax.all_to_all(jnp.stack([down_weight] * lax.axis_size('sp')), 'sp', 0, 0)]
  transfers between devices with their start and end apart: 3 -> 3, of which waited for: 2 -> 2; matrix products, arithmetic and copies ran while one was open for 35% -> 26% of each run, Pallas kernels for 0% -> 0%
where the time goes in v1:
time: 427 us; the launch traced here: 425 us
  waiting for transfers between devices  210 us (49%)
  matrix products  86.4 us (20%)
  blocking collectives  65.5 us (15%)
  other arithmetic  33.7 us (8%)
  between operations  13.7 us (3%)
  starting transfers between devices  10.9 us (3%)
  local copies, waits for them, and re-layouts  4.48 us (1%)
    all_to_all x1, waiting for transfers between devices, body(): lax.all_to_all(jnp.stack([down_weight] * lax.axis_size('sp')), 'sp', 0, 0)  124 us
    all_gather x2, waiting for transfers between devices, in_one_piece(): lax.all_gather(both, axis, axis=dim, tiled=True)  85.3 us
    all_to_all x2, blocking collectives, sum_at_owner(): pieces = lax.all_to_all(split_up(x, dim, size), axis, 0, 0, tiled=True)  34.3 us
    all_to_all x3, blocking collectives, sent_to_all(): return lax.all_to_all(copies, axis, split_axis=0, concat_axis=0, tiled=True)  31.2 us
    dot_general x2, matrix products, update(): jnp.einsum('qhd,khd->hqk', queries[:, :, :plain_dim], key_rows, preferred...  29.7 us
    dot_general x2, matrix products, update(): jnp.einsum('hqk,khd->qhd', raised.astype(jnp.bfloat16), value_rows, prefe...  23.2 us
    reduce_sum x2, other arithmetic, update(): totals = totals * factor + jnp.sum(raised, axis=-1)  16.7 us
    dot_general x2, matrix products, update(): jnp.einsum('qhd,kd->hqk', queries[:, :, plain_dim:], rotary_rows, preferr...  16.2 us
  transfers between devices with their start and end apart: 3, of which 2 were waited for; matrix products, arithmetic and copies ran while one was open for 26% of the time, Pallas kernels for 0%

profile of v1, /device:TPU:8, one launch (start us, length us, event | category | flops | bytes accessed | tf_op | source)
XLA Modules:
  0.0 424.6 jit_solution(5656187371803055865)
XLA Ops:
  6.5 1.1 copy.42
  7.6 1.4 pad_maximum_fusion.4
  9.1 1.6 pad_maximum_fusion.1
  10.7 1.1 fusion.72
  11.8 1.3 convolution_bitcast_fusion.4
  13.2 1.3 convolution_bitcast_fusion.5
  14.6 85.3 %all-gather.3.cloned.1.call-done = bf16[16384,288]{0,1:T(8,128)(2,1)} async-done(((bf16[256,288]{0,1:T(8,128)(2,1)}), bf16[16384,288]{0,1:T(8,128)(2,1)}) %all-gather.3.cloned.1.call-update) | async-done | bytes 9437200 | tf_op jit(solution)/shard_map/all_gather | solution.py:24
  99.9 5.1 %fusion.4 = f32[16384]{0:T(1024)S(1)} fusion(bf16[16384,288]{0,1:T(8,128)(2,1)} %all-gather.3.cloned.1.call-done), kind=kLoop, calls=%fused_computation.14 | loop fusion | flops 12566528 | bytes 8454144 | tf_op jit(solution)/shard_map/reduce_sum | solution.py:84
  105.1 1.4 fusion.62
  106.5 4.4 %fusion.84 = (bf16[16384,8]{0,1:T(8,128)(2,1)S(1)}, bf16[16384,8]{0,1:T(8,128)(2,1)S(1)}, bf16[16384,8]{0,1:T(8,128)(2,1)S(1)}, bf16[16384,8]{0,1:T(8,128)(2,1)S(1)}) fusion(f32[16384,1,32]{0,2,1:T(8,128)S(1)} %fusion.62, f32[8]{0:T(128)S(1)} %multiply_power_fusion, f32[16384]{0:T(1024)S(1)} %get-tuple-element.43, f32[16384]{0:T(1024)S(1)} %get-tuple-element.44), kind=kLoop, calls=%fused_computation.90 | loop fusion | flops 2359296 | bytes 3276832 | tf_op jit(solution)/shard_map/concatenate | solution.py:78
  110.8 8.1 %convolution_bitcast_fusion.2 = f32[1,256,16384]{2,1,0:T(8,128)} fusion(bf16[16384,8]{0,1:T(8,128)(2,1)S(1)} %get-tuple-element.13, bf16[16384,8]{0,1:T(8,128)(2,1)S(1)} %get-tuple-element.14, bf16[16384,8]{0,1:T(8,128)(2,1)S(1)} %get-tuple-element.10, bf16[16384,8]{0,1:T(8,128)(2,1)S(1)} %get-tuple-element.9, bf16[256,1,8]{0,2,1:T(8,128)(2,1)S(1)} %get-tuple-element.25, ...), kind=kOutput, calls=%fused_computation.2 | convolution fusion | flops 272695296 | bytes 17842176 | tf_op jit(solution)/shard_map/qhd,kd->hqk/dot_general | solution.py:109
  118.9 8.1 %convolution_bitcast_fusion = f32[1,256,16384]{2,1,0:T(8,128)} fusion(bf16[16384,8]{0,1:T(8,128)(2,1)S(1)} %get-tuple-element.13, bf16[16384,8]{0,1:T(8,128)(2,1)S(1)} %get-tuple-element.14, bf16[16384,8]{0,1:T(8,128)(2,1)S(1)} %get-tuple-element.10, bf16[16384,8]{0,1:T(8,128)(2,1)S(1)} %get-tuple-element.9, bf16[256,1,8]{0,2,1:T(8,128)(2,1)S(1)} %get-tuple-element.28, ...), kind=kOutput, calls=%fused_computation | convolution fusion | flops 272695296 | bytes 17842176 | tf_op jit(solution)/shard_map/qhd,kd->hqk/dot_general | solution.py:109
  127.0 14.5 %fusion.167 = (f32[256]{0:T(256)S(1)}, f32[1,256,16384]{2,1,0:T(8,128)}) fusion(f32[1,256,16384]{2,1,0:T(8,128)} %convolution_bitcast_fusion.2, bf16[256,64]{0,1:T(8,128)(2,1)S(1)} %copy-done.5, f32[256]{0:T(256)S(1)} %copy-done.6, f32[16384]{0:T(1024)S(1)} %add_rsqrt_fusion, bf16[16384,288]{0,1:T(8,128)(2,1)} %all-gather.3.cloned.1.call-done, ...), kind=kOutput, calls=%fused_computation.191 | convolution fusion | flops 1104150272 | bytes 42076160 | tf_op jit(solution)/shard_map/qhd,khd->hqk/dot_general | solution.py:106
  141.5 8.2 %fusion.7 = f32[256]{0:T(256)S(1)} fusion(f32[1,256,16384]{2,1,0:T(8,128)} %get-tuple-element.42, f32[256]{0:T(256)S(1)} %get-tuple-element.41), kind=kLoop, calls=%fused_computation.19 | loop fusion | flops 8388352 | bytes 16779264 | tf_op jit(solution)/shard_map/reduce_sum | solution.py:116
  149.7 15.2 %fusion.164 = (f32[256]{0:T(256)S(1)}, f32[1,256,16384]{2,1,0:T(8,128)}) fusion(f32[1,256,16384]{2,1,0:T(8,128)} %convolution_bitcast_fusion, bf16[256,128]{1,0:T(8,128)(2,1)S(1)} %copy-done.4, f32[256]{0:T(256)S(1)} %copy-done.6, f32[16384]{0:T(1024)S(1)} %add_rsqrt_fusion, bf16[16384,288]{0,1:T(8,128)(2,1)} %all-gather.3.cloned.1.call-done, ...), kind=kOutput, calls=%fused_computation.190 | convolution fusion | flops 2178940672 | bytes 42141696 | tf_op jit(solution)/shard_map/qhd,khd->hqk/dot_general | solution.py:106
  164.9 8.5 %fusion.9 = f32[256]{0:T(256)S(1)} fusion(f32[1,256,16384]{2,1,0:T(8,128)} %get-tuple-element.40, f32[256]{0:T(256)S(1)} %get-tuple-element.39), kind=kLoop, calls=%fused_computation.21 | loop fusion | flops 8388352 | bytes 16779264 | tf_op jit(solution)/shard_map/reduce_sum | solution.py:116
  173.4 11.9 %fusion.44 = bf16[256,128]{0,1:T(8,128)(2,1)S(1)} fusion(f32[1,256,16384]{2,1,0:T(8,128)} %get-tuple-element.40, f32[256]{0:T(256)S(1)} %get-tuple-element.39, bf16[256,128]{1,0:T(8,128)(2,1)S(1)} %copy-done.11, f32[256]{0:T(256)S(1)} %get-tuple-element.38, f32[256]{0:T(256)S(1)} %get-tuple-element.37, f32[256]{0:T(256)S(1)} %copy-done.6, ...), kind=kOutput, calls=%fused_computation.46 | convolution fusion | flops 2174844928 | bytes 25366528 | tf_op jit(solution)/shard_map/hqk,khd->qhd/dot_general | solution.py:117
  185.4 0.5 fusion.170
  185.9 11.3 %fusion.59 = bf16[256,64]{0,1:T(8,128)(2,1)S(1)} fusion(f32[1,256,16384]{2,1,0:T(8,128)} %get-tuple-element.42, f32[256]{0:T(256)S(1)} %get-tuple-element.41, bf16[256,64]{0,1:T(8,128)(2,1)S(1)} %copy-done.12, f32[256]{0:T(256)S(1)} %get-tuple-element.36, f32[256]{0:T(256)S(1)} %get-tuple-element.35, f32[256]{0:T(256)S(1)} %copy-done.6, ...), kind=kOutput, calls=%fused_computation.51 | convolution fusion | flops 1100005376 | bytes 25300992 | tf_op jit(solution)/shard_map/hqk,khd->qhd/dot_general | solution.py:117
  197.2 0.5 fusion.26
  197.8 18.7 %all_to_all.32 = bf16[4,256,512]{2,1,0:T(8,128)(2,1)S(1)} all-to-all(bf16[4,256,512]{2,1,0:T(8,128)(2,1)S(1)} %bitcast.141), channel_id=1, replica_groups=mesh['sp'=64,'tp'=4] {'tp'}, dimensions={0} | all-to-all | bytes 2097152 | tf_op jit(solution)/shard_map/all_to_all | solution.py:34
  216.6 0.2 fusion.87
  216.8 7.7 %all_to_all.33 = f32[4,1,512]{2,1,0:T(1,128)S(1)} all-to-all(f32[4,1,512]{2,1,0:T(1,128)S(1)} %broadcast_in_dim.16), channel_id=1, replica_groups=mesh['sp'=64,'tp'=4] {'tp'}, dimensions={0} | all-to-all | bytes 16384 | tf_op jit(solution)/shard_map/all_to_all | solution.py:40
  224.9 15.9 %all_to_all.34 = bf16[4,256,512]{1,2,0:T(8,128)(2,1)S(1)} all-to-all(bf16[4,256,512]{1,2,0:T(8,128)(2,1)S(1)} %broadcast_in_dim.17), channel_id=1, replica_groups=mesh['sp'=64,'tp'=4] {'tp'}, dimensions={0} | all-to-all | bytes 2097152 | tf_op jit(solution)/shard_map/all_to_all | solution.py:40
  240.8 3.0 stack.2
  243.8 10.9 %all-to-all-start.3 = ((bf16[64,1408,32]{1,2,0:T(8,128)(2,1)}), bf16[64,1408,32]{1,2,0:T(8,128)(2,1)}, u32[]{:S(2)}, u32[]{:S(2)}) async-start(bf16[64,1408,32]{1,2,0:T(8,128)(2,1)} %stack.2), calls=%async_computation.3 | async-start | bytes 11534336 | tf_op jit(solution)/shard_map/all_to_all | solution.py:222
  254.7 5.6 %fusion.21 = f32[256,1408]{1,0:T(8,128)} fusion(bf16[256,2048]{0,1:T(8,128)(2,1)S(1)} %bitcast.143, bf16[2048,2816]{1,0:T(8,128)(2,1)} %all-gather.5.cloned.1.call-done), kind=kOutput, calls=%fused_computation.31 | convolution fusion | flops 1476395008 | bytes 8257536 | tf_op jit(solution)/shard_map/dot_general | solution.py:216
  260.3 124.5 %all-to-all-done.3 = bf16[64,1408,32]{1,2,0:T(8,128)(2,1)} async-done(((bf16[64,1408,32]{1,2,0:T(8,128)(2,1)}), bf16[64,1408,32]{1,2,0:T(8,128)(2,1)}, u32[]{:S(2)}, u32[]{:S(2)}) %all-to-all-start.3) | async-done | bytes 5767200 | tf_op jit(solution)/shard_map/all_to_all | solution.py:222
  384.8 8.3 %convolution_convert_fusion.4 = bf16[256,2048]{1,0:T(8,128)(2,1)S(1)} fusion(bf16[1408,2048]{0,1:T(8,128)(2,1)} %bitcast.31, bf16[256,2048]{0,1:T(8,128)(2,1)S(1)} %bitcast.144, bf16[2048,2816]{1,0:T(8,128)(2,1)} %all-gather.5.cloned.1.call-done, f32[256,1408]{1,0:T(8,128)} %fusion.21), kind=kOutput, calls=%fused_computation.37 | convolution fusion | flops 2955476992 | bytes 15073280 | tf_op jit(solution)/shard_map/dot_general | solution.py:219
  393.2 15.6 %all_to_all.35 = bf16[4,256,512]{2,1,0:T(8,128)(2,1)S(1)} all-to-all(bf16[4,256,512]{2,1,0:T(8,128)(2,1)S(1)} %bitcast.142), channel_id=1, replica_groups=mesh['sp'=64,'tp'=4] {'tp'}, dimensions={0} | all-to-all | bytes 2097152 | tf_op jit(solution)/shard_map/all_to_all | solution.py:34
  409.2 7.7 %all_to_all.36 = f32[4,1,512]{2,1,0:T(1,128)S(1)} all-to-all(f32[4,1,512]{2,1,0:T(1,128)S(1)} %broadcast_in_dim.18), channel_id=1, replica_groups=mesh['sp'=64,'tp'=4] {'tp'}, dimensions={0} | all-to-all | bytes 16384 | tf_op jit(solution)/shard_map/all_to_all | solution.py:40
  416.9 0.9 add_convert_fusion
  (55 shorter events, 1.5 us)
Async XLA Ops:
  6.5 178.8 %copy-start = (bf16[128,2048]{1,0:T(8,128)(2,1)S(1)}, bf16[128,2048]{1,0:T(8,128)(2,1)}, u32[]{:S(2)}) copy-start(bf16[128,2048]{1,0:T(8,128)(2,1)} %param.34) | copy-start | bytes 1572868
  6.5 93.4 %all-gather.3.cloned.1.call-start = ((), (), s32[]{:S(2)}) async-start(), calls=%async_computation.6 | async-start | bytes 9584640 | tf_op jit(solution)/shard_map/all_gather | solution.py:24
  9.0 245.7 %all-gather.5.cloned.1.call-start = ((), (), s32[]{:S(2)}) async-start(), calls=%async_computation.7 | async-start | bytes 11714560 | tf_op jit(solution)/shard_map/all_gather | solution.py:24
  118.9 8.1 %copy-start.5 = (bf16[256,64]{0,1:T(8,128)(2,1)S(1)}, bf16[256,64]{0,1:T(8,128)(2,1)}, u32[]{:S(2)}) copy-start(bf16[256,64]{0,1:T(8,128)(2,1)} %param.28) | copy-start | bytes 98308
  118.9 8.1 %copy-start.6 = (f32[256]{0:T(256)S(1)}, f32[256]{0:T(256)}, u32[]{:S(2)}) copy-start(f32[256]{0:T(256)} %param.26) | copy-start | bytes 3076
  141.5 8.2 %copy-start.4 = (bf16[256,128]{1,0:T(8,128)(2,1)S(1)}, bf16[256,128]{1,0:T(8,128)(2,1)}, u32[]{:S(2)}) copy-start(bf16[256,128]{1,0:T(8,128)(2,1)} %param.31) | copy-start | bytes 196612
  164.9 8.5 %copy-start.11 = (bf16[256,128]{1,0:T(8,128)(2,1)S(1)}, bf16[256,128]{1,0:T(8,128)(2,1)}, u32[]{:S(2)}) copy-start(bf16[256,128]{1,0:T(8,128)(2,1)} %param.32) | copy-start | bytes 196612
  173.4 12.4 %copy-start.12 = (bf16[256,64]{0,1:T(8,128)(2,1)S(1)}, bf16[256,64]{0,1:T(8,128)(2,1)}, u32[]{:S(2)}) copy-start(bf16[256,64]{0,1:T(8,128)(2,1)} %param.29) | copy-start | bytes 98308
  185.8 11.3 %copy-start.2 = (bf16[64,2048]{1,0:T(8,128)(2,1)S(1)}, bf16[64,2048]{1,0:T(8,128)(2,1)}, u32[]{:S(2)}) copy-start(bf16[64,2048]{1,0:T(8,128)(2,1)} %param.33) | copy-start | bytes 786436
  185.9 30.7 %copy-start.1 = (bf16[256,512]{1,0:T(8,128)(2,1)S(1)}, bf16[256,512]{1,0:T(8,128)(2,1)}, u32[]{:S(2)}) copy-start(bf16[256,512]{1,0:T(8,128)(2,1)} %param.21) | copy-start | bytes 786436
  197.2 27.3 %copy-start.7 = (f32[512]{0:T(512)S(1)}, f32[512]{0:T(512)}, u32[]{:S(2)}) copy-start(f32[512]{0:T(512)} %param.36) | copy-start | bytes 6148
  197.2 27.3 %copy-start.8 = (f32[512]{0:T(512)S(1)}, f32[512]{0:T(512)}, u32[]{:S(2)}) copy-start(f32[512]{0:T(512)} %param.35) | copy-start | bytes 6148
  197.2 43.6 %copy-start.3 = (bf16[1408,32]{0,1:T(8,128)(2,1)S(1)}, bf16[1408,32]{0,1:T(8,128)(2,1)}, u32[]{:S(2)}) copy-start(bf16[1408,32]{0,1:T(8,128)(2,1)} %param.39) | copy-start | bytes 270340
  243.8 141.0 %all-to-all-start.3 = ((bf16[64,1408,32]{1,2,0:T(8,128)(2,1)}), bf16[64,1408,32]{1,2,0:T(8,128)(2,1)}, u32[]{:S(2)}, u32[]{:S(2)}) async-start(bf16[64,1408,32]{1,2,0:T(8,128)(2,1)} %stack.2), calls=%async_computation.3 | async-start | bytes 11534336 | tf_op jit(solution)/shard_map/all_to_all | solution.py:222
  384.8 32.1 %copy-start.9 = (f32[512]{0:T(512)S(1)}, f32[512]{0:T(512)}, u32[]{:S(2)}) copy-start(f32[512]{0:T(512)} %param.41) | copy-start | bytes 6148
  384.8 32.1 %copy-start.10 = (f32[512]{0:T(512)S(1)}, f32[512]{0:T(512)}, u32[]{:S(2)}) copy-start(f32[512]{0:T(512)} %param.40) | copy-start | bytes 6148
Sparse Core Ops, SparseCore 0:
  10.0 89.9 all-gather.2
  102.7 88.5 all-gather.4
